TPU v7x, 32 devices: a whole 2x2x4 slice. The times are simulated.
32 devices in a mesh: grp: 2 (over y), sp: 4 (over z), tp: 4 (over x, core).
Axes of the slice: x: 2, y: 2, z: 4, core: 2. Of those that a mesh axis runs over, the one named last changes fastest.
Arguments:
- stream: bfloat16 [2048, 2048], P(('grp', 'sp'), 'tp'), parts along dimension 0, may hold values from -1.5 to 1.5
- layer_norm_gain: float32 [2, 2048], replicated, may hold values from 0.1 to 1.9
- convolution_in_weight: bfloat16 [2, 2048, 1536], P(None, 'sp', 'tp'), may hold values from -0.125 to 0.125
- gating_in_weight: bfloat16 [2, 2048, 1536], P(None, 'sp', 'tp'), may hold values from -0.125 to 0.125
- output_weight: bfloat16 [2, 1536, 2048], P(None, 'tp', 'sp'), may hold values from -0.15625 to 0.15625
- convolution_kernel_taps: float32 [2, 4, 1536], P(None, None, 'tp'), may hold values from -12 to 12
- recurrent_gate_blocks: bfloat16 [2, 2, 2, 12, 128, 128], P(None, None, None, 'tp'), may hold values from -0.5 to 0.5
- channel_decay_logit: float32 [2, 2, 1536], P(None, None, 'tp')
- position_decay_boost: float32 [2, 2, 2048], P(None, None, ('grp', 'sp')), parts along dimension 2, may hold values from -1.4 to 0, as said below
Outputs:
- new_stream: bfloat16 [2048, 2048], P(('grp', 'sp'), 'tp'), parts along dimension 0
There are 2 independent parts, one for each index of `grp`. A program takes and returns all parts, laid end to end along the dimension named above; an argument that names none is the same for every part. Nothing has to cross between parts.
Inputs may be any that keep to these rules, and one draw needn't show every extreme that they name: `position_decay_boost`: zero at all but a few positions.
All inputs are finite; a program needn't handle non-finite values.
Results may differ from a plain program's by a relative error of at most 0.025.
Values may be sent and summed in bfloat16 or wider, within the bound.
A program may use at most 128 MiB of HBM per device.

v0:
```python
import jax
import jax.numpy as jnp
from jax import lax
from jax.sharding import PartitionSpec as P

EPS = 1e-06
RECURRENT_WIDTH = 8.0


def extended(cells, sides, width):
    for axis, dim in sides:
        count = lax.axis_size(axis)
        ends = count - 1
        head = lax.slice_in_dim(cells, 0, width, axis=dim)
        tail = lax.slice_in_dim(cells, cells.shape[dim] - width, cells.shape[dim], axis=dim)
        cells = jnp.concatenate(
            [
                lax.ppermute(tail, axis, [(i, (i + 1) % count) for i in range(ends)]),
                cells,
                lax.ppermute(head, axis, [((i + 1) % count, i) for i in range(ends)]),
            ],
            axis=dim,
        )
    return cells


def entering(ends, place, count):
    forward = jnp.zeros_like(ends[0, :1])
    backward = forward
    for step in range(count - 1):
        forward = jnp.where(step < place, ends[step, 0:1] * forward + ends[step, 1:2], forward)
        source = count - 1 - step
        backward = jnp.where(
            source > place, ends[source, 2:3] * backward + ends[source, 3:4], backward
        )
    return (forward, backward)


def rms_norm(values, gain_row):
    floats = values.astype(jnp.float32)
    inverse = lax.rsqrt(jnp.mean(floats * floats, axis=-1, keepdims=True) + EPS)
    return (floats * inverse * gain_row).astype(jnp.bfloat16)


def combine_pairs(earlier, latter):
    return (earlier[0] * latter[0], latter[0] * earlier[1] + latter[1])


def local(
    stream,
    layer_norm_gain,
    convolution_in_weight,
    gating_in_weight,
    output_weight,
    convolution_kernel_taps,
    recurrent_gate_blocks,
    channel_decay_logit,
    position_decay_boost,
):
    tok_rows = stream.shape[0]
    channels = convolution_in_weight.shape[2]
    gate_count = recurrent_gate_blocks.shape[3]
    block_width = recurrent_gate_blocks.shape[4]
    seq_devices = lax.axis_size("sp")
    my_index = lax.axis_index("sp")
    seq_length = tok_rows * seq_devices
    positions = my_index * tok_rows + lax.iota(jnp.int32, tok_rows)
    at_first = (positions == 0)[:, None]
    at_last = (positions == seq_length - 1)[:, None]
    for layer_index in range(convolution_in_weight.shape[0]):
        features = lax.all_gather(stream, "tp", axis=1, tiled=True)
        normed = rms_norm(features, layer_norm_gain[layer_index])
        acc_x = jnp.dot(
            normed,
            lax.all_gather(convolution_in_weight[layer_index], "sp", axis=0, tiled=True),
            preferred_element_type=jnp.float32,
        )
        acc_y = jnp.dot(
            normed,
            lax.all_gather(gating_in_weight[layer_index], "sp", axis=0, tiled=True),
            preferred_element_type=jnp.float32,
        )
        proj_x = acc_x.astype(jnp.bfloat16)
        proj_y = acc_y.astype(jnp.bfloat16)
        padded = extended(proj_x, (("sp", 0),), 2).astype(jnp.float32)
        taps_now = convolution_kernel_taps[layer_index]
        conv_mixed = (
            taps_now[0] * padded[1 : tok_rows + 1]
            + taps_now[1] * padded[2 : tok_rows + 2]
            + taps_now[2] * padded[3 : tok_rows + 3]
            + taps_now[3] * padded[4 : tok_rows + 4]
        )
        convolution_output = conv_mixed.astype(jnp.bfloat16)
        conv_float = convolution_output.astype(jnp.float32)
        grouped = convolution_output.reshape(tok_rows, gate_count, block_width)
        results = []
        for scan_direction in range(2):
            gate_matrix_pair = recurrent_gate_blocks[layer_index, scan_direction]
            recurrent_branch = jax.nn.sigmoid(
                jnp.einsum(
                    "tnc,ncd->tnd", grouped, gate_matrix_pair[0], preferred_element_type=jnp.float32
                ).reshape(tok_rows, channels)
            )
            input_gate = jax.nn.sigmoid(
                jnp.einsum(
                    "tnc,ncd->tnd", grouped, gate_matrix_pair[1], preferred_element_type=jnp.float32
                ).reshape(tok_rows, channels)
            )
            decay_logarithm = (
                -RECURRENT_WIDTH
                * jax.nn.softplus(-channel_decay_logit[layer_index, scan_direction])
                * recurrent_branch
                + position_decay_boost[layer_index, scan_direction][:, None]
            )
            is_start = at_first if scan_direction == 0 else at_last
            multiplier = jnp.where(is_start, 1.0, jnp.sqrt(-jnp.expm1(2.0 * decay_logarithm)))
            driven = multiplier * input_gate * conv_float
            results.append(
                lax.associative_scan(
                    combine_pairs,
                    (jnp.exp(decay_logarithm), driven),
                    reverse=scan_direction == 1,
                    axis=0,
                )
            )
        cum_fwd, local_fwd = results[0]
        cum_bwd, local_bwd = results[1]
        ends = jnp.concatenate([cum_fwd[-1:], local_fwd[-1:], cum_bwd[:1], local_bwd[:1]], axis=0)
        enter_fwd, enter_bwd = entering(lax.all_gather(ends, "sp"), my_index, seq_devices)
        state_sum = local_fwd + cum_fwd * enter_fwd + local_bwd + cum_bwd * enter_bwd
        gated = (state_sum * jax.nn.gelu(proj_y.astype(jnp.float32))).astype(jnp.bfloat16)
        partials = jnp.dot(
            gated,
            lax.all_gather(output_weight[layer_index], "sp", axis=1, tiled=True),
            preferred_element_type=jnp.float32,
        ).astype(jnp.bfloat16)
        branch_sum = lax.psum_scatter(
            partials.astype(jnp.float32).astype(jnp.bfloat16), "tp", scatter_dimension=1, tiled=True
        ).astype(jnp.float32)
        stream = (stream.astype(jnp.float32) + branch_sum).astype(jnp.bfloat16)
    return stream


def solution(mesh):
    return jax.shard_map(
        local,
        mesh=mesh,
        in_specs=(
            P(("grp", "sp"), "tp"),
            P(),
            P(None, "sp", "tp"),
            P(None, "sp", "tp"),
            P(None, "tp", "sp"),
            P(None, None, "tp"),
            P(None, None, None, "tp", None, None),
            P(None, None, "tp"),
            P(None, None, ("grp", "sp")),
        ),
        out_specs=P(("grp", "sp"), "tp"),
        check_vma=False,
    )
```

profile of v0, /device:TPU:0, one launch (start us, length us, event | category | flops | bytes accessed | tf_op | source)
XLA Modules:
  0.0 339.8 jit_solution(17607182247680082666)
XLA Ops:
  7.3 2.1 fusion.210
  9.5 1.0 fusion.211
  10.7 1.0 fusion.212
  14.8 13.5 %all-gather.19.cloned.1.call-done = bf16[256,2048]{1,0:T(8,128)(2,1)} async-done(((bf16[256,512]{1,0:T(8,128)(2,1)}), bf16[256,2048]{1,0:T(8,128)(2,1)}) %all-gather.19.cloned.1.call-update) | async-done | bytes 1048592 | tf_op jit(solution)/shard_map/all_gather | solution.py:71
  28.3 1.5 fusion
  29.9 37.1 %all-gather.23.cloned.1.call-done = bf16[1,2048,384]{2,1,0:T(8,128)(2,1)} async-done(((bf16[1,512,384]{2,1,0:T(8,128)(2,1)}), bf16[1,2048,384]{2,1,0:T(8,128)(2,1)}) %all-gather.23.cloned.1.call-update) | async-done | bytes 1572880 | tf_op jit(solution)/shard_map/all_gather | solution.py:75
  67.0 2.5 fusion.40
  69.5 2.6 collective-permute-start
  72.1 1.3 collective-permute-start.1
  74.0 3.6 %collective-permute-done.1 = bf16[2,384]{1,0:T(2,128)(2,1)S(1)} collective-permute-done((bf16[2,384]{1,0:T(2,128)(2,1)S(1)}, bf16[2,384]{1,0:T(2,128)(2,1)S(1)}, u32[]{:S(2)}, u32[]{:S(2)}) %collective-permute-start.1) | collective-permute-done | bytes 1568 | tf_op jit(solution)/shard_map/ppermute | solution.py:20
  80.0 1.6 convert_multiply_fusion.7
  92.4 0.9 pad.453
  94.5 1.0 pad.455
  95.5 0.7 pad_maximum_fusion.3
  96.3 1.0 pad.454
  97.3 0.8 copy-done.6
  98.1 0.8 add.1023
  98.9 4.0 %rev.16 = f32[256,384]{1,0:T(8,128)} reverse(f32[256,384]{1,0:T(8,128)} %add.1023), dimensions={0} | reverse | bytes 786432 | tf_op jit(solution)/shard_map/rev | solution.py:119
  102.8 0.8 add.998
  103.6 3.9 %rev.17 = f32[256,384]{1,0:T(8,128)} reverse(f32[256,384]{1,0:T(8,128)} %add.998), dimensions={0} | reverse | bytes 786432 | tf_op jit(solution)/shard_map/rev | solution.py:119
  107.5 0.7 slice_add_fusion.12
  108.3 13.6 %all-gather.8 = f32[4,4,384]{2,1,0:T(4,128)S(1)} all-gather(f32[1,4,384]{2,1,0:T(4,128)S(1)} %maximum_bitcast_fusion), channel_id=3, replica_groups=mesh['grp'=2,'sp'=4,'tp'=4] {'sp'}, dimensions={0}, use_global_device_ids=true | all-gather | bytes 30720 | tf_op jit(solution)/shard_map/all_gather | solution.py:129
  122.0 20.0 %all-gather.27.cloned.1.call-done = bf16[1,384,2048]{2,1,0:T(8,128)(2,1)} async-done(((bf16[1,384,512]{2,1,0:T(8,128)(2,1)}), bf16[1,384,2048]{2,1,0:T(8,128)(2,1)}) %all-gather.27.cloned.1.call-update) | async-done | bytes 1572880 | tf_op jit(solution)/shard_map/all_gather | solution.py:134
  142.0 4.7 %convolution_convert_fusion.1 = bf16[256,2048]{1,0:T(8,128)(2,1)} fusion(bf16[1,384,2048]{2,1,0:T(8,128)(2,1)} %all-gather.27.cloned.1.call-done, bf16[1,2048,384]{2,1,0:T(8,128)(2,1)} %all-gather.25.cloned.1.call-done, f32[256,384]{1,0:T(8,128)} %rev.17, f32[256,384]{1,0:T(8,128)} %rev.16, f32[256,384]{1,0:T(8,128)S(1)} %pad.422, f32[256,384]{1,0:T(8,128)S(1)} %pad.423, ...), kind=kOutput, calls=%fused_computation.5 | convolution fusion | flops 809795584 | bytes 7614464 | tf_op jit(solution)/shard_map/dot_general | solution.py:132
  146.7 23.7 %reduce-scatter.3.cloned.1.call-done = bf16[256,512]{1,0:T(8,128)(2,1)} async-done(((bf16[256,2048]{1,0:T(8,128)(2,1)}), bf16[256,512]{1,0:T(8,128)(2,1)}) %reduce-scatter.3.cloned.1.call-update) | async-done | bytes 262160 | tf_op jit(solution)/shard_map/reduce_scatter | solution.py:137
  170.5 1.7 add_convert_fusion.1
  174.5 14.5 %all-gather.21.cloned.1.call-done = bf16[256,2048]{1,0:T(8,128)(2,1)} async-done(((bf16[256,512]{1,0:T(8,128)(2,1)}), bf16[256,2048]{1,0:T(8,128)(2,1)}) %all-gather.21.cloned.1.call-update) | async-done | bytes 1048592 | tf_op jit(solution)/shard_map/all_gather | solution.py:71
  189.0 1.5 fusion.3
  190.6 37.1 %all-gather.29.cloned.1.call-done = bf16[1,2048,384]{2,1,0:T(8,128)(2,1)} async-done(((bf16[1,512,384]{2,1,0:T(8,128)(2,1)}), bf16[1,2048,384]{2,1,0:T(8,128)(2,1)}) %all-gather.29.cloned.1.call-update) | async-done | bytes 1572880 | tf_op jit(solution)/shard_map/all_gather | solution.py:75
  227.7 2.5 fusion.49
  230.2 2.6 collective-permute-start.2
  232.8 1.3 collective-permute-start.3
  234.8 3.6 %collective-permute-done.3 = bf16[2,384]{1,0:T(2,128)(2,1)S(1)} collective-permute-done((bf16[2,384]{1,0:T(2,128)(2,1)S(1)}, bf16[2,384]{1,0:T(2,128)(2,1)S(1)}, u32[]{:S(2)}, u32[]{:S(2)}) %collective-permute-start.3) | collective-permute-done | bytes 1568 | tf_op jit(solution)/shard_map/ppermute | solution.py:20
  240.7 1.6 convert_multiply_fusion.5
  252.5 0.9 pad.517
  254.6 1.0 pad.519
  255.6 0.7 pad_maximum_fusion.7
  256.3 1.0 pad.518
  257.4 0.8 copy-done.5
  258.1 0.8 add.1117
  258.9 4.0 %rev.18 = f32[256,384]{1,0:T(8,128)} reverse(f32[256,384]{1,0:T(8,128)} %add.1117), dimensions={0} | reverse | bytes 786432 | tf_op jit(solution)/shard_map/rev | solution.py:119
  262.9 0.8 add.1092
  263.7 3.8 %rev.19 = f32[256,384]{1,0:T(8,128)} reverse(f32[256,384]{1,0:T(8,128)} %add.1092), dimensions={0} | reverse | bytes 786432 | tf_op jit(solution)/shard_map/rev | solution.py:119
  268.3 13.5 %all-gather.9 = f32[4,4,384]{2,1,0:T(4,128)S(1)} all-gather(f32[1,4,384]{2,1,0:T(4,128)S(1)} %maximum_bitcast_fusion.1), channel_id=7, replica_groups=mesh['grp'=2,'sp'=4,'tp'=4] {'sp'}, dimensions={0}, use_global_device_ids=true | all-gather | bytes 30720 | tf_op jit(solution)/shard_map/all_gather | solution.py:129
  281.9 20.9 %all-gather.33.cloned.1.call-done = bf16[1,384,2048]{2,1,0:T(8,128)(2,1)} async-done(((bf16[1,384,512]{2,1,0:T(8,128)(2,1)}), bf16[1,384,2048]{2,1,0:T(8,128)(2,1)}) %all-gather.33.cloned.1.call-update) | async-done | bytes 1572880 | tf_op jit(solution)/shard_map/all_gather | solution.py:134
  302.8 4.7 %convolution_convert_fusion = bf16[256,2048]{1,0:T(8,128)(2,1)} fusion(bf16[1,384,2048]{2,1,0:T(8,128)(2,1)} %all-gather.33.cloned.1.call-done, bf16[1,2048,384]{2,1,0:T(8,128)(2,1)} %all-gather.31.cloned.1.call-done, f32[256,384]{1,0:T(8,128)} %rev.19, f32[256,384]{1,0:T(8,128)} %rev.18, f32[256,384]{1,0:T(8,128)S(1)} %pad.486, f32[256,384]{1,0:T(8,128)S(1)} %pad.487, ...), kind=kOutput, calls=%fused_computation.4 | convolution fusion | flops 809795584 | bytes 7614464 | tf_op jit(solution)/shard_map/dot_general | solution.py:132
  307.4 23.8 %reduce-scatter.5.cloned.1.call-done = bf16[256,512]{1,0:T(8,128)(2,1)} async-done(((bf16[256,2048]{1,0:T(8,128)(2,1)}), bf16[256,512]{1,0:T(8,128)(2,1)}) %reduce-scatter.5.cloned.1.call-update) | async-done | bytes 262160 | tf_op jit(solution)/shard_map/reduce_scatter | solution.py:137
  331.2 1.7 add_convert_fusion
  (646 shorter events, 33.9 us)
Async XLA Ops:
  6.5 3.0 copy-start.8
  6.5 21.8 %all-gather.19.cloned.1.call-start = ((), (), s32[]{:S(2)}) async-start(), calls=%async_computation.2 | async-start | bytes 1310720 | tf_op jit(solution)/shard_map/all_gather | solution.py:71
  7.3 59.7 %all-gather.23.cloned.1.call-start = ((), (), s32[]{:S(2)}) async-start(), calls=%async_computation.6 | async-start | bytes 1966080 | tf_op jit(solution)/shard_map/all_gather | solution.py:75
  9.4 1.3 copy-start.9
  9.4 112.5 %all-gather.25.cloned.1.call-start = ((), (), s32[]{:S(2)}) async-start(), calls=%async_computation.7 | async-start | bytes 1966080 | tf_op jit(solution)/shard_map/all_gather | solution.py:80
  10.5 1.3 copy-start.27
  10.5 1.9 copy-start.28
  10.5 2.5 copy-start.31
  10.5 3.1 copy-start.37
  10.5 131.5 %all-gather.27.cloned.1.call-start = ((), (), s32[]{:S(2)}) async-start(), calls=%async_computation.8 | async-start | bytes 1966080 | tf_op jit(solution)/shard_map/all_gather | solution.py:134
  11.7 158.8 %reduce-scatter.3.cloned.1.call-start = ((), (), s32[]{:S(2)}) async-start(), calls=%async_computation.3 | async-start | bytes 1310720 | tf_op jit(solution)/shard_map/reduce_scatter | solution.py:137
  12.4 57.1 %copy-start.18 = (f32[1,2048]{1,0:T(1,128)}, f32[1,2048]{1,0:T(1,128)S(1)}, u32[]{:S(2)}) copy-start(f32[1,2048]{1,0:T(1,128)S(1)} %get-tuple-element.124) | copy-start | bytes 24580
  13.0 64.7 %copy-start.23 = (f32[384]{0:T(512)}, f32[384]{0:T(512)S(1)}, u32[]{:S(2)}) copy-start(f32[384]{0:T(512)S(1)} %get-tuple-element.27) | copy-start | bytes 4612
  13.0 64.7 %copy-start.24 = (f32[384]{0:T(512)}, f32[384]{0:T(512)S(1)}, u32[]{:S(2)}) copy-start(f32[384]{0:T(512)S(1)} %get-tuple-element.28) | copy-start | bytes 4612
  13.0 64.7 %copy-start.25 = (f32[384]{0:T(512)}, f32[384]{0:T(512)S(1)}, u32[]{:S(2)}) copy-start(f32[384]{0:T(512)S(1)} %get-tuple-element.29) | copy-start | bytes 4612
  13.0 64.7 %copy-start.26 = (f32[384]{0:T(512)}, f32[384]{0:T(512)S(1)}, u32[]{:S(2)}) copy-start(f32[384]{0:T(512)S(1)} %get-tuple-element.30) | copy-start | bytes 4612
  29.9 39.6 %copy-start.35 = (f32[256]{0:T(256)}, f32[256]{0:T(256)S(1)}, u32[]{:S(2)}) copy-start(f32[256]{0:T(256)S(1)} %add_rsqrt_fusion.1) | copy-start | bytes 3076
  69.5 8.6 %copy-start.38 = (bf16[2,2,2,3,128,128]{5,4,3,2,1,0:T(8,128)(2,1)S(1)}, bf16[2,2,2,3,128,128]{5,4,3,2,1,0:T(8,128)(2,1)}, u32[]{:S(2)}) copy-start(bf16[2,2,2,3,128,128]{5,4,3,2,1,0:T(8,128)(2,1)} %param.15) | copy-start | bytes 2359300
  69.5 4.5 %collective-permute-start = (bf16[2,384]{1,0:T(2,128)(2,1)S(1)}, bf16[2,384]{1,0:T(2,128)(2,1)S(1)}, u32[]{:S(2)}, u32[]{:S(2)}) collective-permute-start(bf16[2,384]{1,0:T(2,128)(2,1)S(1)} %get-tuple-element.73), channel_id=1, source_target_pairs={{0,4},{4,8},{8,12},{1,5},{5,9},{9,13},{2,6},{6,10},{10,14},{3,7},{... | collective-permute-start | bytes 4616 | tf_op jit(solution)/shard_map/ppermute | solution.py:18
  72.1 5.5 %collective-permute-start.1 = (bf16[2,384]{1,0:T(2,128)(2,1)S(1)}, bf16[2,384]{1,0:T(2,128)(2,1)S(1)}, u32[]{:S(2)}, u32[]{:S(2)}) collective-permute-start(bf16[2,384]{1,0:T(2,128)(2,1)S(1)} %get-tuple-element.74), channel_id=1, source_target_pairs={{4,0},{8,4},{12,8},{5,1},{9,5},{13,9},{6,2},{10,6},{14,10},{7,3},{... | collective-permute-start | bytes 4616 | tf_op jit(solution)/shard_map/ppermute | solution.py:20
  89.9 1.6 copy-start.10
  95.5 1.8 copy-start.4
  98.9 43.1 %copy-start = (bf16[256,2048]{1,0:T(8,128)(2,1)S(1)}, bf16[256,2048]{1,0:T(8,128)(2,1)}, u32[]{:S(2)}) copy-start(bf16[256,2048]{1,0:T(8,128)(2,1)} %all-gather.19.cloned.1.call-done) | copy-start | bytes 3145732
  98.9 43.1 %copy-start.19 = (f32[1,2048]{1,0:T(1,128)S(1)}, f32[1,2048]{1,0:T(1,128)}, u32[]{:S(2)}) copy-start(f32[1,2048]{1,0:T(1,128)} %copy-done.18) | copy-start | bytes 24580
  98.9 43.1 %copy-start.36 = (f32[256]{0:T(256)S(1)}, f32[256]{0:T(256)}, u32[]{:S(2)}) copy-start(f32[256]{0:T(256)} %copy-done.35) | copy-start | bytes 3076
  121.9 48.5 %copy-start.7 = (bf16[256,512]{1,0:T(8,128)(2,1)S(1)}, bf16[256,512]{1,0:T(8,128)(2,1)}, u32[]{:S(2)}) copy-start(bf16[256,512]{1,0:T(8,128)(2,1)} %param.9) | copy-start | bytes 786436
  146.7 81.0 %copy-start.16 = (f32[1,2048]{1,0:T(1,128)S(1)}, f32[1,2048]{1,0:T(1,128)}, u32[]{:S(2)}) copy-start(f32[1,2048]{1,0:T(1,128)} %get-tuple-element.123) | copy-start | bytes 24580
  146.7 42.3 %all-gather.21.cloned.1.call-start = ((), (), s32[]{:S(2)}) async-start(), calls=%async_computation.4 | async-start | bytes 1310720 | tf_op jit(solution)/shard_map/all_gather | solution.py:71
  172.2 55.5 %all-gather.29.cloned.1.call-start = ((), (), s32[]{:S(2)}) async-start(), calls=%async_computation.9 | async-start | bytes 1966080 | tf_op jit(solution)/shard_map/all_gather | solution.py:75
  172.9 108.9 %all-gather.31.cloned.1.call-start = ((), (), s32[]{:S(2)}) async-start(), calls=%async_computation.10 | async-start | bytes 1966080 | tf_op jit(solution)/shard_map/all_gather | solution.py:80
  173.7 129.1 %all-gather.33.cloned.1.call-start = ((), (), s32[]{:S(2)}) async-start(), calls=%async_computation.11 | async-start | bytes 1966080 | tf_op jit(solution)/shard_map/all_gather | solution.py:134
  174.4 156.8 %reduce-scatter.5.cloned.1.call-start = ((), (), s32[]{:S(2)}) async-start(), calls=%async_computation.5 | async-start | bytes 1310720 | tf_op jit(solution)/shard_map/reduce_scatter | solution.py:137
  190.5 39.6 %copy-start.33 = (f32[256]{0:T(256)}, f32[256]{0:T(256)S(1)}, u32[]{:S(2)}) copy-start(f32[256]{0:T(256)S(1)} %add_rsqrt_fusion) | copy-start | bytes 3076
  227.7 6.5 %copy-start.29 = (f32[384]{0:T(512)S(1)}, f32[384]{0:T(512)}, u32[]{:S(2)}) copy-start(f32[384]{0:T(512)} %get-tuple-element.33) | copy-start | bytes 4612
  227.7 6.5 %copy-start.30 = (f32[384]{0:T(512)S(1)}, f32[384]{0:T(512)}, u32[]{:S(2)}) copy-start(f32[384]{0:T(512)} %get-tuple-element.36) | copy-start | bytes 4612
  227.7 10.7 %copy-start.20 = (f32[384]{0:T(512)S(1)}, f32[384]{0:T(512)}, u32[]{:S(2)}) copy-start(f32[384]{0:T(512)} %get-tuple-element.26) | copy-start | bytes 4612
  227.7 10.7 %copy-start.21 = (f32[384]{0:T(512)S(1)}, f32[384]{0:T(512)}, u32[]{:S(2)}) copy-start(f32[384]{0:T(512)} %get-tuple-element.31) | copy-start | bytes 4612
  227.7 10.7 %copy-start.22 = (f32[384]{0:T(512)S(1)}, f32[384]{0:T(512)}, u32[]{:S(2)}) copy-start(f32[384]{0:T(512)} %get-tuple-element.32) | copy-start | bytes 4612
  230.2 8.6 %copy-start.39 = (bf16[2,2,2,3,128,128]{5,4,3,2,1,0:T(8,128)(2,1)S(1)}, bf16[2,2,2,3,128,128]{5,4,3,2,1,0:T(8,128)(2,1)}, u32[]{:S(2)}) copy-start(bf16[2,2,2,3,128,128]{5,4,3,2,1,0:T(8,128)(2,1)} %param.15) | copy-start | bytes 2359300
  230.2 4.6 %collective-permute-start.2 = (bf16[2,384]{1,0:T(2,128)(2,1)S(1)}, bf16[2,384]{1,0:T(2,128)(2,1)S(1)}, u32[]{:S(2)}, u32[]{:S(2)}) collective-permute-start(bf16[2,384]{1,0:T(2,128)(2,1)S(1)} %get-tuple-element.61), channel_id=1, source_target_pairs={{0,4},{4,8},{8,12},{1,5},{5,9},{9,13},{2,6},{6,10},{10,14},{3,7},{... | collective-permute-start | bytes 4616 | tf_op jit(solution)/shard_map/ppermute | solution.py:18
  232.8 5.5 %collective-permute-start.3 = (bf16[2,384]{1,0:T(2,128)(2,1)S(1)}, bf16[2,384]{1,0:T(2,128)(2,1)S(1)}, u32[]{:S(2)}, u32[]{:S(2)}) collective-permute-start(bf16[2,384]{1,0:T(2,128)(2,1)S(1)} %get-tuple-element.62), channel_id=1, source_target_pairs={{4,0},{8,4},{12,8},{5,1},{9,5},{13,9},{6,2},{10,6},{14,10},{7,3},{... | collective-permute-start | bytes 4616 | tf_op jit(solution)/shard_map/ppermute | solution.py:20
  250.0 1.6 copy-start.11
  251.4 0.9 copy-start.15
  255.6 1.8 copy-start.3
  258.9 43.8 %copy-start.1 = (bf16[256,2048]{1,0:T(8,128)(2,1)S(1)}, bf16[256,2048]{1,0:T(8,128)(2,1)}, u32[]{:S(2)}) copy-start(bf16[256,2048]{1,0:T(8,128)(2,1)} %all-gather.21.cloned.1.call-done) | copy-start | bytes 3145732
  258.9 43.8 %copy-start.17 = (f32[1,2048]{1,0:T(1,128)S(1)}, f32[1,2048]{1,0:T(1,128)}, u32[]{:S(2)}) copy-start(f32[1,2048]{1,0:T(1,128)} %get-tuple-element.123) | copy-start | bytes 24580
  258.9 43.8 %copy-start.34 = (f32[256]{0:T(256)S(1)}, f32[256]{0:T(256)}, u32[]{:S(2)}) copy-start(f32[256]{0:T(256)} %copy-done.33) | copy-start | bytes 3076
  281.9 49.4 %copy-start.2 = (bf16[256,512]{1,0:T(8,128)(2,1)S(1)}, bf16[256,512]{1,0:T(8,128)(2,1)}, u32[]{:S(2)}) copy-start(bf16[256,512]{1,0:T(8,128)(2,1)} %add_convert_fusion.1) | copy-start | bytes 786436
  (6 other events, 5.0 us)
Sparse Core Ops, SparseCore 0:
  8.9 19.4 all-gather.18
  29.9 37.0 all-gather.22
  68.5 35.8 all-gather.24
  105.9 36.0 all-gather.26
  146.8 23.6 reduce-scatter.2
  172.3 16.6 all-gather.20
  190.6 37.0 all-gather.28
  229.2 35.8 all-gather.30
  266.7 35.9 all-gather.32
  307.6 23.6 reduce-scatter.4
where the time goes:
time: 341 us; the launch traced here: 340 us
  waiting for transfers between devices  201 us (59%)
  local copies, waits for them, and re-layouts  42.5 us (12%)
  other arithmetic  27.8 us (8%)
  blocking collectives  27 us (8%)
  between operations  16.9 us (5%)
  matrix products  16.7 us (5%)
  starting transfers between devices  8.38 us (2%)
    all_gather x2, waiting for transfers between devices, local(): lax.all_gather(convolution_in_weight[layer_index], 'sp', axis=0, tiled=True)  74.2 us
    reduce_scatter x2, waiting for transfers between devices, local(): lax.psum_scatter(partials.astype(jnp.float32).astype(jnp.bfloat16), 'tp',...  47.5 us
    all_gather x2, waiting for transfers between devices, local(): lax.all_gather(output_weight[layer_index], 'sp', axis=1, tiled=True)  40.9 us
    all_gather x2, waiting for transfers between devices, local(): features = lax.all_gather(stream, 'tp', axis=1, tiled=True)  28.1 us
    all_gather x2, blocking collectives, local(): lax.all_gather(ends, 'sp')  27 us
    rev x4, local copies, waits for them, and re-layouts, local(): lax.associative_scan(combine_pairs, (jnp.exp(decay_logarithm), driven), r...  15.6 us
    add x68, other arithmetic, local(): lax.associative_scan(combine_pairs, (jnp.exp(decay_logarithm), driven), r...  10.5 us
    dot_general x2, matrix products, local(): jnp.dot(gated, lax.all_gather(output_weight[layer_index], 'sp', axis=1, t...  9.31 us
  transfers between devices with their start and end apart: 14, of which 10 were waited for; matrix products, arithmetic and copies ran while one was open for 21% of the time, Pallas kernels for 0%

commit v1 on v0

--- a/solution.py
+++ b/solution.py
@@ -68,7 +68,14 @@
     at_first = (positions == 0)[:, None]
     at_last = (positions == seq_length - 1)[:, None]
     for layer_index in range(convolution_in_weight.shape[0]):
-        features = lax.all_gather(stream, "tp", axis=1, tiled=True)
+        ring = [stream]
+        for hop in range(3):
+            ring.append(lax.ppermute(ring[-1], "tp", [(dev, (dev + 1) % 4) for dev in range(4)]))
+        features = jnp.roll(
+            jnp.concatenate(ring[::-1], axis=1),
+            (lax.axis_index("tp") + 1) * ring[0].shape[1],
+            axis=1,
+        )
         normed = rms_norm(features, layer_norm_gain[layer_index])
         acc_x = jnp.dot(
             normed,

time: 341 us -> 436 us (1.28)
  local copies, waits for them, and re-layouts: 42.5 us -> 149 us
  waiting for transfers between devices: 201 us -> 122 us
  other arithmetic: 27.8 us -> 84.8 us
  matrix products: 16.7 us -> 23.3 us
    slice x220, local copies, waits for them, and re-layouts: 8.85 us -> 91.2 us  [local(): lax.associative_scan(combine_pairs, (jnp.exp(decay_logarithm), driven), r...]
    all_gather x2, waiting for transfers between devices: 40.9 us -> 0.04 us  [local(): lax.all_gather(output_weight[layer_index], 'sp', axis=1, tiled=True)]
    all_gather x2, waiting for transfers between devices: 74.2 us -> 35 us  [local(): lax.all_gather(convolution_in_weight[layer_index], 'sp', axis=0, tiled=True)]
    ppermute x0 -> x6, waiting for transfers between devices: none -> 31.1 us  [local(): lax.ppermute(ring[-1], 'tp', [(dev, (dev + 1) % 4) for dev in range(4)])]
    all_gather x2 -> x0, waiting for transfers between devices: 28.1 us -> none  [local(): features = lax.all_gather(stream, 'tp', axis=1, tiled=True)]
    pad x112, local copies, waits for them, and re-layouts: 7.85 us -> 29.4 us  [local(): lax.associative_scan(combine_pairs, (jnp.exp(decay_logarithm), driven), r...]
    add x52, other arithmetic: 2.3 us -> 22.6 us  [combine_pairs(): return (earlier[0] * latter[0], latter[0] * earlier[1] + latter[1])]
    concatenate x56, other arithmetic: 2.07 us -> 19.9 us  [local(): lax.associative_scan(combine_pairs, (jnp.exp(decay_logarithm), driven), r...]
  transfers between devices with their start and end apart: 14 -> 18, of which waited for: 10 -> 12; matrix products, arithmetic and copies ran while one was open for 21% -> 57% of each run, Pallas kernels for 0% -> 0%
where the time goes in v1:
time: 436 us; the launch traced here: 431 us
  local copies, waits for them, and re-layouts  149 us (34%)
  waiting for transfers between devices  122 us (28%)
  other arithmetic  84.8 us (19%)
  blocking collectives  26.3 us (6%)
  matrix products  23.3 us (5%)
  between operations  16.6 us (4%)
  starting transfers between devices  8.86 us (2%)
    slice x220, local copies, waits for them, and re-layouts, local(): lax.associative_scan(combine_pairs, (jnp.exp(decay_logarithm), driven), r...  91.2 us
    reduce_scatter x2, waiting for transfers between devices, local(): lax.psum_scatter(partials.astype(jnp.float32).astype(jnp.bfloat16), 'tp',...  46.5 us
    all_gather x2, waiting for transfers between devices, local(): lax.all_gather(convolution_in_weight[layer_index], 'sp', axis=0, tiled=True)  35 us
    ppermute x6, waiting for transfers between devices, local(): lax.ppermute(ring[-1], 'tp', [(dev, (dev + 1) % 4) for dev in range(4)])  31.1 us
    pad x112, local copies, waits for them, and re-layouts, local(): lax.associative_scan(combine_pairs, (jnp.exp(decay_logarithm), driven), r...  29.4 us
    all_gather x2, blocking collectives, local(): lax.all_gather(ends, 'sp')  26.3 us
    add x68, other arithmetic, local(): lax.associative_scan(combine_pairs, (jnp.exp(decay_logarithm), driven), r...  24.8 us
    add x52, other arithmetic, combine_pairs(): return (earlier[0] * latter[0], latter[0] * earlier[1] + latter[1])  22.6 us
  transfers between devices with their start and end apart: 18, of which 12 were waited for; matrix products, arithmetic and copies ran while one was open for 57% of the time, Pallas kernels for 0%

profile of v1, /device:TPU:0, one launch (start us, length us, event | category | flops | bytes accessed | tf_op | source)
XLA Modules:
  0.0 431.2 jit_solution(11274290968168247839)
XLA Ops:
  6.5 2.2 fusion.226
  12.0 4.3 %collective-permute-done = bf16[256,512]{1,0:T(8,128)(2,1)S(1)} collective-permute-done((bf16[256,512]{1,0:T(8,128)(2,1)S(1)}, bf16[256,512]{1,0:T(8,128)(2,1)S(1)}, u32[]{:S(2)}, u32[]{:S(2)}) %collective-permute-start) | collective-permute-done | bytes 262176 | tf_op jit(solution)/shard_map/ppermute | solution.py:73
  17.6 4.6 %collective-permute-done.1 = bf16[256,512]{1,0:T(8,128)(2,1)S(1)} collective-permute-done((bf16[256,512]{1,0:T(8,128)(2,1)S(1)}, bf16[256,512]{1,0:T(8,128)(2,1)S(1)}, u32[]{:S(2)}, u32[]{:S(2)}) %collective-permute-start.1) | collective-permute-done | bytes 262176 | tf_op jit(solution)/shard_map/ppermute | solution.py:73
  22.8 5.2 %collective-permute-done.2 = bf16[256,512]{1,0:T(8,128)(2,1)S(1)} collective-permute-done((bf16[256,512]{1,0:T(8,128)(2,1)S(1)}, bf16[256,512]{1,0:T(8,128)(2,1)S(1)}, u32[]{:S(2)}, u32[]{:S(2)}) %collective-permute-start.2) | collective-permute-done | bytes 262176 | tf_op jit(solution)/shard_map/ppermute | solution.py:73
  28.0 2.8 fusion
  30.8 17.8 %all-gather.17.cloned.1.call-done = bf16[1,2048,384]{2,1,0:T(8,128)(2,1)} async-done(((bf16[1,512,384]{2,1,0:T(8,128)(2,1)}), bf16[1,2048,384]{2,1,0:T(8,128)(2,1)}) %all-gather.17.cloned.1.call-update) | async-done | bytes 1572880 | tf_op jit(solution)/shard_map/all_gather | solution.py:82
  48.7 2.2 fusion.40
  50.9 2.5 collective-permute-start.3
  53.4 1.5 collective-permute-start.4
  54.9 3.9 collective-permute-done.4
  67.1 2.1 convert_multiply_fusion.7
  125.4 1.6 pad.439
  127.1 2.4 slice.1364
  129.5 2.4 slice.1406
  132.6 1.8 fusion.140
  134.5 2.5 pad.455
  137.0 1.7 pad_maximum_fusion.3
  138.6 2.6 pad.454
  141.3 1.9 add.1036
  143.2 3.9 rev.16
  147.9 3.9 rev.17
  152.5 13.2 %all-gather.8 = f32[4,4,384]{2,1,0:T(4,128)S(1)} all-gather(f32[1,4,384]{2,1,0:T(4,128)S(1)} %maximum_bitcast_fusion), channel_id=3, replica_groups=mesh['grp'=2,'sp'=4,'tp'=4] {'sp'}, dimensions={0}, use_global_device_ids=true | all-gather | bytes 30720 | tf_op jit(solution)/shard_map/all_gather | solution.py:136
  165.8 4.7 %convolution_convert_fusion.1 = bf16[256,2048]{1,0:T(8,128)(2,1)} fusion(bf16[1,384,2048]{2,1,0:T(8,128)(2,1)} %all-gather.21.cloned.1.call-done, bf16[1,2048,384]{2,1,0:T(8,128)(2,1)} %all-gather.19.cloned.1.call-done, f32[256,384]{1,0:T(8,128)} %rev.17, f32[256,384]{1,0:T(8,128)} %rev.16, f32[256,384]{1,0:T(8,128)S(1)} %pad.422, f32[256,384]{1,0:T(8,128)S(1)} %pad.423, ...), kind=kOutput, calls=%fused_computation.5 | convolution fusion | flops 809795584 | bytes 7614464 | tf_op jit(solution)/shard_map/dot_general | solution.py:139
  171.8 22.6 %reduce-scatter.3.cloned.1.call-done = bf16[256,512]{1,0:T(8,128)(2,1)} async-done(((bf16[256,2048]{1,0:T(8,128)(2,1)}), bf16[256,512]{1,0:T(8,128)(2,1)}) %reduce-scatter.3.cloned.1.call-update) | async-done | bytes 262160 | tf_op jit(solution)/shard_map/reduce_scatter | solution.py:144
  195.5 5.8 %collective-permute-done.5 = bf16[256,512]{1,0:T(8,128)(2,1)S(1)} collective-permute-done((bf16[256,512]{1,0:T(8,128)(2,1)S(1)}, bf16[256,512]{1,0:T(8,128)(2,1)S(1)}, u32[]{:S(2)}, u32[]{:S(2)}) %collective-permute-start.5) | collective-permute-done | bytes 262176 | tf_op jit(solution)/shard_map/ppermute | solution.py:73
  201.3 5.8 %collective-permute-done.6 = bf16[256,512]{1,0:T(8,128)(2,1)S(1)} collective-permute-done((bf16[256,512]{1,0:T(8,128)(2,1)S(1)}, bf16[256,512]{1,0:T(8,128)(2,1)S(1)}, u32[]{:S(2)}, u32[]{:S(2)}) %collective-permute-start.6) | collective-permute-done | bytes 262176 | tf_op jit(solution)/shard_map/ppermute | solution.py:73
  207.4 5.5 %collective-permute-done.7 = bf16[256,512]{1,0:T(8,128)(2,1)S(1)} collective-permute-done((bf16[256,512]{1,0:T(8,128)(2,1)S(1)}, bf16[256,512]{1,0:T(8,128)(2,1)S(1)}, u32[]{:S(2)}, u32[]{:S(2)}) %collective-permute-start.7) | collective-permute-done | bytes 262176 | tf_op jit(solution)/shard_map/ppermute | solution.py:73
  212.9 2.8 fusion.3
  215.8 17.2 %all-gather.23.cloned.1.call-done = bf16[1,2048,384]{2,1,0:T(8,128)(2,1)} async-done(((bf16[1,512,384]{2,1,0:T(8,128)(2,1)}), bf16[1,2048,384]{2,1,0:T(8,128)(2,1)}) %all-gather.23.cloned.1.call-update) | async-done | bytes 1572880 | tf_op jit(solution)/shard_map/all_gather | solution.py:82
  233.0 2.2 fusion.49
  235.2 2.5 collective-permute-start.8
  239.0 4.1 collective-permute-done.9
  252.2 2.3 convert_multiply_fusion.5
  264.2 1.5 multiply_add_fusion.13
  339.3 2.1 pad.499
  351.4 1.6 pad.470
  353.1 1.6 pad.503
  356.5 2.4 slice.1556
  362.1 1.6 pad.502
  365.4 2.5 pad.518
  367.9 1.8 add.1130
  369.7 3.9 rev.18
  373.6 1.8 add.1105
  375.5 3.9 rev.19
  380.8 13.2 %all-gather.9 = f32[4,4,384]{2,1,0:T(4,128)S(1)} all-gather(f32[1,4,384]{2,1,0:T(4,128)S(1)} %maximum_bitcast_fusion.1), channel_id=7, replica_groups=mesh['grp'=2,'sp'=4,'tp'=4] {'sp'}, dimensions={0}, use_global_device_ids=true | all-gather | bytes 30720 | tf_op jit(solution)/shard_map/all_gather | solution.py:136
  394.1 4.6 %convolution_convert_fusion = bf16[256,2048]{1,0:T(8,128)(2,1)} fusion(bf16[1,384,2048]{2,1,0:T(8,128)(2,1)} %all-gather.27.cloned.1.call-done, bf16[1,2048,384]{2,1,0:T(8,128)(2,1)} %all-gather.25.cloned.1.call-done, f32[256,384]{1,0:T(8,128)} %rev.19, f32[256,384]{1,0:T(8,128)} %rev.18, f32[256,384]{1,0:T(8,128)S(1)} %pad.486, f32[256,384]{1,0:T(8,128)S(1)} %pad.487, ...), kind=kOutput, calls=%fused_computation.4 | convolution fusion | flops 809795584 | bytes 7614464 | tf_op jit(solution)/shard_map/dot_general | solution.py:139
  398.8 23.8 %reduce-scatter.5.cloned.1.call-done = bf16[256,512]{1,0:T(8,128)(2,1)} async-done(((bf16[256,2048]{1,0:T(8,128)(2,1)}), bf16[256,512]{1,0:T(8,128)(2,1)}) %reduce-scatter.5.cloned.1.call-update) | async-done | bytes 262160 | tf_op jit(solution)/shard_map/reduce_scatter | solution.py:144
  422.6 1.7 add_convert_fusion
  (778 shorter events, 184.2 us)
Async XLA Ops:
  6.5 42.1 %all-gather.17.cloned.1.call-start = ((), (), s32[]{:S(2)}) async-start(), calls=%async_computation.4 | async-start | bytes 1966080 | tf_op jit(solution)/shard_map/all_gather | solution.py:82
  8.7 157.1 %all-gather.19.cloned.1.call-start = ((), (), s32[]{:S(2)}) async-start(), calls=%async_computation.5 | async-start | bytes 1966080 | tf_op jit(solution)/shard_map/all_gather | solution.py:87
  9.8 156.0 %all-gather.21.cloned.1.call-start = ((), (), s32[]{:S(2)}) async-start(), calls=%async_computation.6 | async-start | bytes 1966080 | tf_op jit(solution)/shard_map/all_gather | solution.py:141
  9.9 6.5 %collective-permute-start = (bf16[256,512]{1,0:T(8,128)(2,1)S(1)}, bf16[256,512]{1,0:T(8,128)(2,1)S(1)}, u32[]{:S(2)}, u32[]{:S(2)}) collective-permute-start(bf16[256,512]{1,0:T(8,128)(2,1)S(1)} %copy-done.4), channel_id=1, source_target_pairs={{0,1},{1,2},{2,3},{3,0},{4,5},{5,6},{6,7},{7,4},{8,9},{9,10},{10,1... | collective-permute-start | bytes 786440 | tf_op jit(solution)/shard_map/ppermute | solution.py:73
  11.4 183.1 %reduce-scatter.3.cloned.1.call-start = ((), (), s32[]{:S(2)}) async-start(), calls=%async_computation.2 | async-start | bytes 1310720 | tf_op jit(solution)/shard_map/reduce_scatter | solution.py:144
  12.0 38.8 %copy-start.41 = (f32[1,2048]{1,0:T(1,128)}, f32[1,2048]{1,0:T(1,128)S(1)}, u32[]{:S(2)}) copy-start(f32[1,2048]{1,0:T(1,128)S(1)} %get-tuple-element.129) | copy-start | bytes 24580
  16.4 5.8 %collective-permute-start.1 = (bf16[256,512]{1,0:T(8,128)(2,1)S(1)}, bf16[256,512]{1,0:T(8,128)(2,1)S(1)}, u32[]{:S(2)}, u32[]{:S(2)}) collective-permute-start(bf16[256,512]{1,0:T(8,128)(2,1)S(1)} %collective-permute-done), channel_id=1, source_target_pairs={{0,1},{1,2},{2,3},{3,0},{4,5},{5,6},{6,7},{7,4},{8,9},{9,10},{10,1... | collective-permute-start | bytes 786440 | tf_op jit(solution)/shard_map/ppermute | solution.py:73
  22.2 5.8 %collective-permute-start.2 = (bf16[256,512]{1,0:T(8,128)(2,1)S(1)}, bf16[256,512]{1,0:T(8,128)(2,1)S(1)}, u32[]{:S(2)}, u32[]{:S(2)}) collective-permute-start(bf16[256,512]{1,0:T(8,128)(2,1)S(1)} %collective-permute-done.1), channel_id=1, source_target_pairs={{0,1},{1,2},{2,3},{3,0},{4,5},{5,6},{6,7},{7,4},{8,9},{9,10},{10,1... | collective-permute-start | bytes 786440 | tf_op jit(solution)/shard_map/ppermute | solution.py:73
  30.8 20.0 %copy-start.94 = (f32[256]{0:T(256)}, f32[256]{0:T(256)S(1)}, u32[]{:S(2)}) copy-start(f32[256]{0:T(256)S(1)} %add_rsqrt_fusion.1) | copy-start | bytes 3076
  50.9 4.0 collective-permute-start.3
  53.4 5.5 %collective-permute-start.4 = (bf16[2,384]{1,0:T(2,128)(2,1)S(1)}, bf16[2,384]{1,0:T(2,128)(2,1)S(1)}, u32[]{:S(2)}, u32[]{:S(2)}) collective-permute-start(bf16[2,384]{1,0:T(2,128)(2,1)S(1)} %get-tuple-element.79), channel_id=1, source_target_pairs={{4,0},{8,4},{12,8},{5,1},{9,5},{13,9},{6,2},{10,6},{14,10},{7,3},{... | collective-permute-start | bytes 4616 | tf_op jit(solution)/shard_map/ppermute | solution.py:20
  89.8 12.5 %copy-start.69 = (f32[1,384]{1,0:T(1,128)S(1)}, f32[1,384]{1,0:T(1,128)}, u32[]{:S(2)}) copy-start(f32[1,384]{1,0:T(1,128)} %slice.1649) | copy-start | bytes 4612
  89.9 12.5 %copy-start.67 = (f32[1,384]{1,0:T(1,128)S(1)}, f32[1,384]{1,0:T(1,128)}, u32[]{:S(2)}) copy-start(f32[1,384]{1,0:T(1,128)} %slice.1623) | copy-start | bytes 4612
  143.2 22.7 %copy-start.42 = (f32[1,2048]{1,0:T(1,128)S(1)}, f32[1,2048]{1,0:T(1,128)}, u32[]{:S(2)}) copy-start(f32[1,2048]{1,0:T(1,128)} %copy-done.41) | copy-start | bytes 24580
  143.2 22.7 %copy-start.95 = (f32[256]{0:T(256)S(1)}, f32[256]{0:T(256)}, u32[]{:S(2)}) copy-start(f32[256]{0:T(256)} %copy-done.94) | copy-start | bytes 3076
  170.6 23.9 %copy-start.5 = (bf16[256,512]{1,0:T(8,128)(2,1)S(1)}, bf16[256,512]{1,0:T(8,128)(2,1)}, u32[]{:S(2)}) copy-start(bf16[256,512]{1,0:T(8,128)(2,1)} %param.11) | copy-start | bytes 786436
  170.6 62.3 %all-gather.23.cloned.1.call-start = ((), (), s32[]{:S(2)}) async-start(), calls=%async_computation.7 | async-start | bytes 1966080 | tf_op jit(solution)/shard_map/all_gather | solution.py:82
  171.2 222.9 %all-gather.25.cloned.1.call-start = ((), (), s32[]{:S(2)}) async-start(), calls=%async_computation.8 | async-start | bytes 1966080 | tf_op jit(solution)/shard_map/all_gather | solution.py:87
  171.8 61.2 %copy-start.39 = (f32[1,2048]{1,0:T(1,128)S(1)}, f32[1,2048]{1,0:T(1,128)}, u32[]{:S(2)}) copy-start(f32[1,2048]{1,0:T(1,128)} %get-tuple-element.128) | copy-start | bytes 24580
  171.8 222.3 %all-gather.27.cloned.1.call-start = ((), (), s32[]{:S(2)}) async-start(), calls=%async_computation.9 | async-start | bytes 1966080 | tf_op jit(solution)/shard_map/all_gather | solution.py:141
  195.5 5.8 %collective-permute-start.5 = (bf16[256,512]{1,0:T(8,128)(2,1)S(1)}, bf16[256,512]{1,0:T(8,128)(2,1)S(1)}, u32[]{:S(2)}, u32[]{:S(2)}) collective-permute-start(bf16[256,512]{1,0:T(8,128)(2,1)S(1)} %add_convert_fusion.1), channel_id=1, source_target_pairs={{0,1},{1,2},{2,3},{3,0},{4,5},{5,6},{6,7},{7,4},{8,9},{9,10},{10,1... | collective-permute-start | bytes 786440 | tf_op jit(solution)/shard_map/ppermute | solution.py:73
  201.3 5.8 %collective-permute-start.6 = (bf16[256,512]{1,0:T(8,128)(2,1)S(1)}, bf16[256,512]{1,0:T(8,128)(2,1)S(1)}, u32[]{:S(2)}, u32[]{:S(2)}) collective-permute-start(bf16[256,512]{1,0:T(8,128)(2,1)S(1)} %collective-permute-done.5), channel_id=1, source_target_pairs={{0,1},{1,2},{2,3},{3,0},{4,5},{5,6},{6,7},{7,4},{8,9},{9,10},{10,1... | collective-permute-start | bytes 786440 | tf_op jit(solution)/shard_map/ppermute | solution.py:73
  207.1 5.8 %collective-permute-start.7 = (bf16[256,512]{1,0:T(8,128)(2,1)S(1)}, bf16[256,512]{1,0:T(8,128)(2,1)S(1)}, u32[]{:S(2)}, u32[]{:S(2)}) collective-permute-start(bf16[256,512]{1,0:T(8,128)(2,1)S(1)} %collective-permute-done.6), channel_id=1, source_target_pairs={{0,1},{1,2},{2,3},{3,0},{4,5},{5,6},{6,7},{7,4},{8,9},{9,10},{10,1... | collective-permute-start | bytes 786440 | tf_op jit(solution)/shard_map/ppermute | solution.py:73
  207.2 215.5 %reduce-scatter.5.cloned.1.call-start = ((), (), s32[]{:S(2)}) async-start(), calls=%async_computation.3 | async-start | bytes 1310720 | tf_op jit(solution)/shard_map/reduce_scatter | solution.py:144
  215.8 19.4 %copy-start.92 = (f32[256]{0:T(256)}, f32[256]{0:T(256)S(1)}, u32[]{:S(2)}) copy-start(f32[256]{0:T(256)S(1)} %add_rsqrt_fusion) | copy-start | bytes 3076
  235.2 3.8 collective-permute-start.8
  237.7 5.5 %collective-permute-start.9 = (bf16[2,384]{1,0:T(2,128)(2,1)S(1)}, bf16[2,384]{1,0:T(2,128)(2,1)S(1)}, u32[]{:S(2)}, u32[]{:S(2)}) collective-permute-start(bf16[2,384]{1,0:T(2,128)(2,1)S(1)} %get-tuple-element.67), channel_id=1, source_target_pairs={{4,0},{8,4},{12,8},{5,1},{9,5},{13,9},{6,2},{10,6},{14,10},{7,3},{... | collective-permute-start | bytes 4616 | tf_op jit(solution)/shard_map/ppermute | solution.py:20
  308.6 13.4 %copy-start.86 = (f32[1,384]{1,0:T(1,128)S(1)}, f32[1,384]{1,0:T(1,128)}, u32[]{:S(2)}) copy-start(f32[1,384]{1,0:T(1,128)} %get-tuple-element.150) | copy-start | bytes 4612
  308.6 13.4 %copy-start.87 = (f32[1,384]{1,0:T(1,128)S(1)}, f32[1,384]{1,0:T(1,128)}, u32[]{:S(2)}) copy-start(f32[1,384]{1,0:T(1,128)} %get-tuple-element.151) | copy-start | bytes 4612
  308.6 13.4 %copy-start.54 = (f32[2,384]{1,0:T(2,128)S(1)}, f32[2,384]{1,0:T(2,128)}, u32[]{:S(2)}) copy-start(f32[2,384]{1,0:T(2,128)} %pad_add_fusion.2) | copy-start | bytes 9220
  308.6 13.5 %copy-start.56 = (f32[2,384]{1,0:T(2,128)S(1)}, f32[2,384]{1,0:T(2,128)}, u32[]{:S(2)}) copy-start(f32[2,384]{1,0:T(2,128)} %pad_add_fusion.3) | copy-start | bytes 9220
  308.6 13.5 %copy-start.82 = (f32[1,384]{1,0:T(1,128)S(1)}, f32[1,384]{1,0:T(1,128)}, u32[]{:S(2)}) copy-start(f32[1,384]{1,0:T(1,128)} %get-tuple-element.148) | copy-start | bytes 4612
  308.7 13.5 %copy-start.83 = (f32[1,384]{1,0:T(1,128)S(1)}, f32[1,384]{1,0:T(1,128)}, u32[]{:S(2)}) copy-start(f32[1,384]{1,0:T(1,128)} %get-tuple-element.149) | copy-start | bytes 4612
  308.7 13.5 %copy-start.45 = (f32[3,384]{1,0:T(4,128)S(1)}, f32[3,384]{1,0:T(4,128)}, u32[]{:S(2)}) copy-start(f32[3,384]{1,0:T(4,128)} %slice.1486) | copy-start | bytes 13828
  308.7 13.5 %copy-start.79 = (f32[1,384]{1,0:T(1,128)S(1)}, f32[1,384]{1,0:T(1,128)}, u32[]{:S(2)}) copy-start(f32[1,384]{1,0:T(1,128)} %slice.1773) | copy-start | bytes 4612
  308.7 13.6 %copy-start.77 = (f32[1,384]{1,0:T(1,128)S(1)}, f32[1,384]{1,0:T(1,128)}, u32[]{:S(2)}) copy-start(f32[1,384]{1,0:T(1,128)} %slice.1747) | copy-start | bytes 4612
  308.8 13.6 %copy-start.37 = (f32[7,384]{1,0:T(8,128)S(1)}, f32[7,384]{1,0:T(8,128)}, u32[]{:S(2)}) copy-start(f32[7,384]{1,0:T(8,128)} %slice.1463) | copy-start | bytes 32260
  308.8 13.6 %copy-start.38 = (f32[7,384]{1,0:T(8,128)S(1)}, f32[7,384]{1,0:T(8,128)}, u32[]{:S(2)}) copy-start(f32[7,384]{1,0:T(8,128)} %slice.1488) | copy-start | bytes 32260
  308.8 13.6 %copy-start.75 = (f32[1,384]{1,0:T(1,128)S(1)}, f32[1,384]{1,0:T(1,128)}, u32[]{:S(2)}) copy-start(f32[1,384]{1,0:T(1,128)} %slice.1772) | copy-start | bytes 4612
  308.8 13.7 %copy-start.73 = (f32[1,384]{1,0:T(1,128)S(1)}, f32[1,384]{1,0:T(1,128)}, u32[]{:S(2)}) copy-start(f32[1,384]{1,0:T(1,128)} %slice.1746) | copy-start | bytes 4612
  308.9 13.7 %copy-start.30 = (f32[15,384]{1,0:T(8,128)S(1)}, f32[15,384]{1,0:T(8,128)}, u32[]{:S(2)}) copy-start(f32[15,384]{1,0:T(8,128)} %slice.1490) | copy-start | bytes 69124
  308.9 13.7 %copy-start.70 = (f32[1,384]{1,0:T(1,128)S(1)}, f32[1,384]{1,0:T(1,128)}, u32[]{:S(2)}) copy-start(f32[1,384]{1,0:T(1,128)} %slice.1771) | copy-start | bytes 4612
  308.9 13.7 %copy-start.68 = (f32[1,384]{1,0:T(1,128)S(1)}, f32[1,384]{1,0:T(1,128)}, u32[]{:S(2)}) copy-start(f32[1,384]{1,0:T(1,128)} %slice.1745) | copy-start | bytes 4612
  309.0 13.7 %copy-start.26 = (f32[31,384]{1,0:T(8,128)S(1)}, f32[31,384]{1,0:T(8,128)}, u32[]{:S(2)}) copy-start(f32[31,384]{1,0:T(8,128)} %slice.1492) | copy-start | bytes 142852
  309.2 13.6 %copy-start.91 = (f32[1,384]{1,0:T(1,128)S(1)}, f32[1,384]{1,0:T(1,128)}, u32[]{:S(2)}) copy-start(f32[1,384]{1,0:T(1,128)} %slice.1770) | copy-start | bytes 4612
  323.7 13.4 %copy-start.27 = (f32[31,384]{1,0:T(8,128)S(1)}, f32[31,384]{1,0:T(8,128)}, u32[]{:S(2)}) copy-start(f32[31,384]{1,0:T(8,128)} %slice.1551) | copy-start | bytes 142852
  369.7 24.4 %copy-start.40 = (f32[1,2048]{1,0:T(1,128)S(1)}, f32[1,2048]{1,0:T(1,128)}, u32[]{:S(2)}) copy-start(f32[1,2048]{1,0:T(1,128)} %get-tuple-element.128) | copy-start | bytes 24580
  369.7 24.4 %copy-start.93 = (f32[256]{0:T(256)S(1)}, f32[256]{0:T(256)}, u32[]{:S(2)}) copy-start(f32[256]{0:T(256)} %copy-done.92) | copy-start | bytes 3076
  (73 other events, 479.1 us)
Sparse Core Ops, SparseCore 0:
  8.9 39.7 all-gather.16
  50.2 35.8 all-gather.18
  87.7 35.8 all-gather.20
  170.7 23.6 reduce-scatter.2
  195.9 37.0 all-gather.22
  234.4 35.8 all-gather.24
  271.9 35.8 all-gather.26
  398.9 23.6 reduce-scatter.4
